TPU v7x, 32 devices: a whole 2x2x4 slice. The times are simulated.
32 devices in a mesh: sp: 8 (over z, y), tp: 4 (over x, core).
Axes of the slice: x: 2, y: 2, z: 4, core: 2. Of those that a mesh axis runs over, the one named last changes fastest.
Arguments:
- layer_input: bfloat16 [6144, 2048], P('sp', 'tp'), may hold values from -6 to 6
- input_norm_gain: bfloat16 [2048], replicated, may hold values from 0.099609375 to 1.8984375
- query_weight: bfloat16 [2048, 2048], P(None, 'tp'), may hold values from -0.125 to 0.125
- forget_weight: bfloat16 [2048, 2048], P(None, 'tp'), may hold values from -0.125 to 0.125
- value_matrix: bfloat16 [2048, 2048], P(None, 'tp'), may hold values from -0.125 to 0.125
- output_gate_weight: bfloat16 [2048, 2048], P(None, 'tp'), may hold values from -0.125 to 0.125
- after_gate_weight: bfloat16 [2048, 2048], P(None, 'tp'), may hold values from -0.125 to 0.125
- before_gate_weight: bfloat16 [2048, 2048], P(None, 'tp'), may hold values from -0.125 to 0.125
- convolution_input_weight: bfloat16 [2048, 2048], P(None, 'tp'), may hold values from -0.125 to 0.125
- forget_minimum: float32 [2048], P('tp'), may hold values from 0.95 to 0.9999837
- surge_log_decay: float32 [6144, 2048], P('sp', 'tp'), may hold values from -2.2 to 0
- convolution_kernel: bfloat16 [3, 2048], P(None, 'tp'), may hold values from -4 to 4
- head_norm_gain: bfloat16 [128], replicated, may hold values from 0.099609375 to 1.8984375
- starting_state: float32 [16, 128, 128], P('tp', 'sp'), may hold values from -0.09375 to 0.09375
- recurrence_output_weight: bfloat16 [2048, 2048], P('tp'), may hold values from -0.09375 to 0.09375
- convolution_output_weight: bfloat16 [2048, 2048], P('tp'), may hold values from -0.09375 to 0.09375
- output_norm_gain: bfloat16 [2048], replicated, may hold values from 0.099609375 to 1.8984375
Outputs:
- layer_out: bfloat16 [6144, 2048], P(('sp', 'tp'))
All inputs are finite; a program needn't handle non-finite values.
Results may differ from a plain program's by a relative error of at most 0.014.
Values may be sent and summed in bfloat16 or wider, within the bound.
A program may use at most 128 MiB of HBM per device.

v0:
```python
import jax
import jax.numpy as jnp
from jax import lax
from jax.sharding import PartitionSpec as P

DK = 128
DV = 128
CK = 3
BLK = 64


EPS = 1e-06
PRECISE_PRODUCT = lax.Precision.HIGHEST


def from_behind(value, axis, by):
    peers = lax.axis_size(axis)
    pairs = [(i, i + by) for i in range(peers) if 0 <= i + by < peers]
    return lax.ppermute(value, axis, pairs)


def rms_scale(value_rows):
    return lax.rsqrt(jnp.mean(value_rows * value_rows, axis=-1, keepdims=True) + EPS)


def block_pass(carry, inputs):
    latent_state, running = carry
    query_rows, key_inputs, value_rows, forget_gate_logits = inputs
    cumulative_decay = jnp.cumsum(forget_gate_logits, axis=1)
    length = query_rows.shape[1]
    causal_masking = jnp.tril(jnp.ones((length, length), dtype=bool))[None, :, :]
    query_scaled_rows = query_rows * jnp.exp(cumulative_decay)
    scaled_key = key_inputs * jnp.exp(-cumulative_decay)
    crossed_output = jnp.einsum(
        "bqy,byx->bqx", query_scaled_rows, latent_state, precision=PRECISE_PRODUCT
    )
    scores = jnp.einsum("htk,hsk->hts", query_scaled_rows, scaled_key, precision=PRECISE_PRODUCT)
    scores = jnp.where(causal_masking, scores, 0.0)
    o_intra = jnp.einsum("hts,hsv->htv", scores, value_rows, precision=PRECISE_PRODUCT)
    block_total = cumulative_decay[:, -1, :]
    latent_state = jnp.exp(block_total)[..., None] * latent_state + jnp.einsum(
        "otm,ote->ome",
        scaled_key * jnp.exp(block_total)[:, None, :],
        value_rows,
        precision=PRECISE_PRODUCT,
    )
    shifted = query_scaled_rows * jnp.exp(running)[:, None, :]
    return ((latent_state, running + block_total), (o_intra + crossed_output, shifted))


def shards(
    layer_input,
    input_norm_gain,
    query_weight,
    forget_weight,
    value_matrix,
    output_gate_weight,
    after_gate_weight,
    before_gate_weight,
    convolution_input_weight,
    forget_minimum,
    surge_log_decay,
    convolution_kernel,
    head_norm_gain,
    starting_state,
    recurrence_output_weight,
    convolution_output_weight,
    output_norm_gain,
):
    tokens_dev = layer_input.shape[0]
    heads_local = query_weight.shape[1] // DK
    blocks = tokens_dev // BLK
    weight_list = (
        query_weight,
        forget_weight,
        value_matrix,
        output_gate_weight,
        after_gate_weight,
        before_gate_weight,
        convolution_input_weight,
    )
    collected_rows = lax.all_gather(layer_input, "tp", axis=1, tiled=True)
    rows_f = collected_rows.astype(jnp.float32)
    normed = (rows_f * rms_scale(rows_f) * input_norm_gain.astype(jnp.float32)).astype(jnp.bfloat16)
    projections = tuple(
        (
            jnp.dot(normed, weight, preferred_element_type=jnp.float32).astype(jnp.bfloat16)
            for weight in weight_list
        )
    )
    query_raw, forget_raw, value_raw, outgate_raw, postgate_raw, pregate_raw, convval_raw = (
        projections
    )
    forget_single = forget_raw.astype(jnp.float32)
    forget_gate_logits = (
        jnp.logaddexp(
            jnp.log(forget_minimum), jnp.log1p(-forget_minimum) + jax.nn.log_sigmoid(forget_single)
        )
        + surge_log_decay
    )
    key_inputs = (1.0 - forget_minimum) * jax.nn.sigmoid(-forget_single)
    query_rows = jax.nn.silu(query_raw.astype(jnp.float32)) * DK ** (-0.5)

    def to_blocks(value_rows, width):
        return value_rows.reshape(blocks, BLK, heads_local, width).transpose(0, 2, 1, 3)

    zero_state = jnp.zeros((heads_local, DK, DV), jnp.float32)
    zero_total = jnp.zeros((heads_local, DK), jnp.float32)
    (local_state, local_total), (partial_output, shifted_query) = lax.scan(
        block_pass,
        (zero_state, zero_total),
        (
            to_blocks(query_rows, DK),
            to_blocks(key_inputs, DK),
            to_blocks(value_raw.astype(jnp.float32), DV),
            to_blocks(forget_gate_logits, DK),
        ),
    )
    moved_state, moved_total = (
        lax.all_to_all(local_state[None], "sp", split_axis=2, concat_axis=0, tiled=True),
        lax.all_to_all(
            local_total[None, :, :, None], "sp", split_axis=2, concat_axis=0, tiled=True
        ),
    )

    def advance(running, item):
        piece_state, piece_total = item
        return (jnp.exp(piece_total) * running + piece_state, running)

    _, entering = lax.scan(advance, starting_state, (moved_state, moved_total))
    carried_state = lax.all_to_all(entering, "sp", split_axis=0, concat_axis=2, tiled=True)[0]
    recurrence_step = partial_output + jnp.einsum(
        "aoxq,oqu->aoxu", shifted_query, carried_state, precision=PRECISE_PRODUCT
    )
    recurrence_step = recurrence_step.transpose(0, 2, 1, 3).reshape(tokens_dev, heads_local, DV)
    normed_heads = recurrence_step * rms_scale(recurrence_step) * head_norm_gain.astype(jnp.float32)
    rec_out = (
        normed_heads.reshape(tokens_dev, heads_local * DV)
        * jax.nn.silu(outgate_raw.astype(jnp.float32))
    ).astype(jnp.bfloat16)
    mixed_in = pregate_raw.astype(jnp.float32) * convval_raw.astype(jnp.float32)
    rim_rows = from_behind(mixed_in[tokens_dev - (CK - 1) :], "sp", 1)
    padded = jnp.concatenate([rim_rows, mixed_in], axis=0)
    taps_f = convolution_kernel.astype(jnp.float32)
    conv_sum = padded[0:tokens_dev] * taps_f[0]
    for offset in range(1, CK):
        conv_sum = conv_sum + padded[offset : offset + tokens_dev] * taps_f[offset]
    conv_out = (postgate_raw.astype(jnp.float32) * conv_sum).astype(jnp.bfloat16)
    mixed = lax.psum_scatter(
        jnp.dot(rec_out, recurrence_output_weight, preferred_element_type=jnp.float32)
        + jnp.dot(conv_out, convolution_output_weight, preferred_element_type=jnp.float32),
        "tp",
        scatter_dimension=0,
        tiled=True,
    )
    return (mixed * rms_scale(mixed) * output_norm_gain.astype(jnp.float32)).astype(jnp.bfloat16)


def solution(mesh):
    return jax.shard_map(
        shards,
        mesh=mesh,
        in_specs=(
            P("sp", "tp"),
            P(),
            P(None, "tp"),
            P(None, "tp"),
            P(None, "tp"),
            P(None, "tp"),
            P(None, "tp"),
            P(None, "tp"),
            P(None, "tp"),
            P("tp"),
            P("sp", "tp"),
            P(None, "tp"),
            P(),
            P("tp", "sp", None),
            P("tp", None),
            P("tp", None),
            P(),
        ),
        out_specs=P(("sp", "tp"), None),
        check_vma=False,
    )
```

profile of v0, /device:TPU:0, one launch (start us, length us, event | category | flops | bytes accessed | tf_op | source)
XLA Modules:
  0.0 328.3 jit_solution(12126143635630605461)
XLA Ops:
  10.1 30.0 %all-gather.2.cloned.1.call-done = bf16[768,2048]{1,0:T(8,128)(2,1)} async-done(((bf16[768,512]{1,0:T(8,128)(2,1)}), bf16[768,2048]{1,0:T(8,128)(2,1)}) %all-gather.2.cloned.1.call-update) | async-done | bytes 3145744 | tf_op jit(solution)/shard_map/all_gather | solution.py:82
  40.2 2.7 fusion.18
  43.0 7.2 %fusion.35 = (f32[768,512]{1,0:T(8,128)}, f32[768,512]{1,0:T(8,128)}) fusion(f32[512]{0:T(512)S(1)} %get-tuple-element.155, f32[768,512]{1,0:T(8,128)} %param.31, f32[512]{0:T(512)S(1)} %get-tuple-element.157, f32[512]{0:T(512)S(1)} %get-tuple-element.156, bf16[2048,512]{1,0:T(8,128)(2,1)} %param.24, bf16[768,2048]{1,0:T(8,128)(2,1)S(1)} %copy-done.5, ...), kind=kOutput, calls=%fused_computation.62 | convolution fusion | flops 1625948160 | bytes 9978880 | tf_op jit(solution)/shard_map/dot_general | solution.py:87
  50.2 2.7 reshape.89
  52.9 2.8 reshape.90
  55.6 5.8 %fusion.39 = f32[768,512]{1,0:T(8,128)} fusion(bf16[2048,512]{1,0:T(8,128)(2,1)} %param.23, bf16[768,2048]{1,0:T(8,128)(2,1)} %all-gather.2.cloned.1.call-done, f32[2048]{0:T(1024)S(1)} %convert_element_type.68, f32[768]{0:T(1024)S(1)} %add_rsqrt_fusion.1), kind=kOutput, calls=%fused_computation.66 | convolution fusion | flops 1619656704 | bytes 6827008 | tf_op jit(solution)/shard_map/dot_general | solution.py:87
  61.4 2.8 reshape.92
  64.1 5.5 %fusion.50 = f32[768,512]{1,0:T(8,128)} fusion(bf16[2048,512]{1,0:T(8,128)(2,1)} %param.25, bf16[768,2048]{1,0:T(8,128)(2,1)} %all-gather.2.cloned.1.call-done, f32[2048]{0:T(1024)S(1)} %convert_element_type.68, f32[768]{0:T(1024)S(1)} %add_rsqrt_fusion.1), kind=kOutput, calls=%fused_computation.95 | convolution fusion | flops 1617690624 | bytes 6827008 | tf_op jit(solution)/shard_map/dot_general | solution.py:87
  69.7 2.7 reshape.94
  72.4 4.2 %copy_bitcast_fusion.2 = (f32[12,4,64,128]{3,2,1,0:T(8,128)}, f32[12,4,64,128]{3,2,1,0:T(8,128)}) fusion(f32[12,64,4,128]{3,2,1,0:T(4,128)} %reshape.90, f32[12,64,4,128]{3,2,1,0:T(4,128)} %reshape.89), kind=kLoop, calls=%fused_computation.81 | loop fusion | bytes 6291456 | tf_op jit(solution)/shard_map/transpose | solution.py:105
  76.6 2.1 copy_bitcast_fusion
  78.7 105.6 %while.30 = (s32[]{:T(128)}, f32[4,128,128]{2,1,0:T(8,128)S(1)}, f32[4,128]{1,0:T(4,128)S(1)}, f32[12,4,64,128]{3,2,0,1:T(8,128)}, f32[12,4,64,128]{3,2,0,1:T(8,...) while((s32[]{:T(128)}, f32[4,128,128]{2,1,0:T(8,128)S(1)}, ...), condition=%wide.region_3.4_spmd.clone, body=%wide.region_1.3_spmd.clone.sunk | while | flops 153670656 | bytes 3577993 | solution.py:109
  83.9 2.0 fusion.91
  92.7 2.0 fusion.91
  110.3 2.0 fusion.91
  154.3 2.0 fusion.91
  171.9 2.0 fusion.91
  180.7 1.9 fusion.91
  185.0 5.5 %all-to-all-start = ((f32[1,4,128,1]{1,3,0,2:T(1,128)}), f32[1,4,128,1]{1,3,0,2:T(1,128)S(1)}, u32[]{:S(2)}, u32[]{:S(2)}) async-start(f32[1,4,128,1]{1,3,0,2:T(1,128)} %bitcast.7), calls=%async_computation | async-start | bytes 131072 | tf_op jit(solution)/shard_map/all_to_all | solution.py:121
  191.5 6.0 %all-to-all-done = f32[1,4,128,1]{1,3,0,2:T(1,128)S(1)} async-done(((f32[1,4,128,1]{1,3,0,2:T(1,128)}), f32[1,4,128,1]{1,3,0,2:T(1,128)S(1)}, u32[]{:S(2)}, u32[]{:S(2)}) %all-to-all-start) | async-done | bytes 2080 | tf_op jit(solution)/shard_map/all_to_all | solution.py:121
  197.5 3.6 %all-to-all-start.1 = ((f32[1,4,128,128]{3,1,0,2:T(4,128)}), f32[1,4,128,128]{3,1,0,2:T(4,128)S(1)}, u32[]{:S(2)}, u32[]{:S(2)}) async-start(f32[1,4,128,128]{3,1,0,2:T(4,128)} %bitcast.111), calls=%async_computation.1 | async-start | bytes 524288 | tf_op jit(solution)/shard_map/all_to_all | solution.py:120
  201.1 4.4 %convolution_convert_fusion = bf16[768,512]{1,0:T(8,128)(2,1)S(1)} fusion(bf16[2048,512]{1,0:T(8,128)(2,1)} %param.29, bf16[768,2048]{1,0:T(8,128)(2,1)} %all-gather.2.cloned.1.call-done, f32[2048]{0:T(1024)S(1)} %convert_element_type.68, f32[768]{0:T(1024)S(1)} %add_rsqrt_fusion.1), kind=kOutput, calls=%fused_computation.89 | convolution fusion | flops 1617297408 | bytes 6040576 | tf_op jit(solution)/shard_map/dot_general | solution.py:87
  205.6 3.6 %all-to-all-done.1 = f32[1,4,128,128]{3,1,0,2:T(4,128)S(1)} async-done(((f32[1,4,128,128]{3,1,0,2:T(4,128)}), f32[1,4,128,128]{3,1,0,2:T(4,128)S(1)}, u32[]{:S(2)}, u32[]{:S(2)}) %all-to-all-start.1) | async-done | bytes 262176 | tf_op jit(solution)/shard_map/all_to_all | solution.py:120
  209.2 5.7 %while.29 = (s32[]{:T(128)}, f32[4,16,128]{2,1,0:T(8,128)S(1)}, f32[8,4,16,128]{3,2,1,0:T(8,128)}, f32[8,4,16,1]{2,1,3,0:T(4,128)S(1)}, f32[8,4,16,128]{3,2,1,0:T(8,128)S(1)}, /*index=5*/s32[]{:T(128)}) while((s32[]{:T(128)}, f32[4,16,128]{2,1,0:T(8,128)S(1)}, f32[8,4,16,128]{3,2,1,0:T(8,128)}, f32[8,4,16,1]{2,1,3,0:T(4,128)S(1)}, ...), condition=%wide.region_5.6_spmd, body=%wide.region_4.5_spmd.sunk | while | flops 16386 | bytes 165197 | solution.py:130
  214.9 3.4 %all-to-all-start.2 = ((f32[8,4,16,128]{3,2,1,0:T(8,128)}), f32[8,4,16,128]{3,2,1,0:T(8,128)S(1)}, u32[]{:S(2)}, u32[]{:S(2)}) async-start(f32[8,4,16,128]{3,2,1,0:T(8,128)} %get-tuple-element.85), calls=%async_computation.2 | async-start | bytes 524288 | tf_op jit(solution)/shard_map/all_to_all | solution.py:131
  218.4 4.4 %convert_multiply_fusion.4 = f32[768,512]{1,0:T(8,128)S(1)} fusion(bf16[768,512]{1,0:T(8,128)(2,1)S(1)} %convolution_convert_fusion, bf16[2048,512]{1,0:T(8,128)(2,1)} %param.28, bf16[768,2048]{1,0:T(8,128)(2,1)} %all-gather.2.cloned.1.call-done, f32[2048]{0:T(1024)S(1)} %convert_element_type.68, f32[768]{0:T(1024)S(1)} %add_rsqrt_fusion.1), kind=kOutput, calls=%fused_computation.85 | convolution fusion | flops 1618477056 | bytes 7613440 | tf_op jit(solution)/shard_map/dot_general | solution.py:87
  223.9 3.9 %collective-permute-start = (f32[2,512]{1,0:T(2,128)S(1)}, f32[2,512]{1,0:T(2,128)S(1)}, u32[]{:S(2)}, u32[]{:S(2)}) collective-permute-start(f32[2,512]{1,0:T(2,128)S(1)} %slice.29), channel_id=1, source_target_pairs={{0,4},{4,8},{8,12},{12,16},{16,20},{20,24},{24,28},{1,5},{5,9},{9,... | collective-permute-start | bytes 12296 | tf_op jit(solution)/shard_map/ppermute | solution.py:19
  227.8 4.5 %multiply_reduce_fusion.1 = (f32[12,64,4]{1,0,2:T(8,128)S(1)}, f32[12,64,4,128]{3,1,0,2:T(8,128)}) fusion(f32[12,4,64,128]{3,2,0,1:T(8,128)} %get-tuple-element.82, f32[4,128,128,1]{2,1,3,0:T(8,128)S(1)} %bitcast.147, f32[12,4,64,128]{3,2,0,1:T(8,128)} %get-tuple-element.86), kind=kOutput, calls=%fused_computation.86 | convolution fusion | flops 605156352 | bytes 4993024 | tf_op jit(solution)/shard_map/aoxq,oqu->aoxu/dot_general | solution.py:132
  232.5 3.6 %copy.52 = f32[12,64,4,128]{3,2,1,0:T(4,128)} copy(f32[12,64,4,128]{3,1,0,2:T(8,128)} %get-tuple-element.159) | data formatting | bytes 3145728 | tf_op jit(solution)/shard_map/transpose | solution.py:135
  237.9 9.8 %fusion.51 = f32[768,2048]{1,0:T(8,128)} fusion(bf16[512,2048]{1,0:T(8,128)(2,1)S(1)} %copy-done, f32[96,8,4,128]{3,2,1,0:T(4,128)} %bitcast.145, f32[96,8,4,128]{3,2,1,0:T(4,128)} %bitcast.144, bf16[2048,512]{1,0:T(8,128)(2,1)} %param.26, f32[512]{0:T(512)S(1)} %broadcast_bitcast_fusion, bf16[768,2048]{1,0:T(8,128)(2,1)} %all-gather.2.cloned.1.call-done, ...), kind=kOutput, calls=%fused_computation.97 | convolution fusion | flops 3231449088 | bytes 16790528 | tf_op jit(solution)/shard_map/dot_general | solution.py:150
  247.7 12.7 %convolution_add_fusion.2 = f32[768,2048]{1,0:T(8,128)} fusion(f32[768,2048]{1,0:T(8,128)} %fusion.51, bf16[512,2048]{1,0:T(8,128)(2,1)} %param.36, f32[2,512]{1,0:T(2,128)S(1)} %collective-permute-done, f32[768,512]{1,0:T(8,128)} %copy-done.7, bf16[2048,512]{1,0:T(8,128)(2,1)} %param.27, f32[512]{0:T(512)S(1)} %bitcast.157, f32[512]{0:T(512)S(1)} %bitcast.156, ...), kind=kOutput, calls=%fused_computation.39 | convolution fusion | flops 3233415168 | bytes 21517312 | tf_op jit(solution)/shard_map/dot_general | solution.py:151
  261.1 57.4 %reduce-scatter.2.cloned.1.call-done = f32[192,2048]{1,0:T(8,128)} async-done(((f32[768,2048]{1,0:T(8,128)}), f32[192,2048]{1,0:T(8,128)}) %reduce-scatter.2.cloned.1.call-update) | async-done | bytes 1572880 | tf_op jit(solution)/shard_map/reduce_scatter | solution.py:149
  (184 shorter events, 111.2 us)
Async XLA Ops:
  6.5 231.4 %copy-start = (bf16[512,2048]{1,0:T(8,128)(2,1)S(1)}, bf16[512,2048]{1,0:T(8,128)(2,1)}, u32[]{:S(2)}) copy-start(bf16[512,2048]{1,0:T(8,128)(2,1)} %param.35) | copy-start | bytes 6291460
  6.5 33.6 %all-gather.2.cloned.1.call-start = ((), (), s32[]{:S(2)}) async-start(), calls=%async_computation.4 | async-start | bytes 3932160 | tf_op jit(solution)/shard_map/all_gather | solution.py:82
  40.2 2.8 copy-start.5
  72.4 4.2 %copy-start.2 = (f32[12,64,4,128]{3,2,1,0:T(4,128)S(1)}, f32[12,64,4,128]{3,2,1,0:T(4,128)}, u32[]{:S(2)}) copy-start(f32[12,64,4,128]{3,2,1,0:T(4,128)} %reshape.92) | copy-start | bytes 4718596
  72.4 4.2 %copy-start.3 = (f32[12,64,4,128]{3,2,1,0:T(4,128)S(1)}, f32[12,64,4,128]{3,2,1,0:T(4,128)}, u32[]{:S(2)}) copy-start(f32[12,64,4,128]{3,2,1,0:T(4,128)} %reshape.94) | copy-start | bytes 4718596
  185.0 12.4 %all-to-all-start = ((f32[1,4,128,1]{1,3,0,2:T(1,128)}), f32[1,4,128,1]{1,3,0,2:T(1,128)S(1)}, u32[]{:S(2)}, u32[]{:S(2)}) async-start(f32[1,4,128,1]{1,3,0,2:T(1,128)} %bitcast.7), calls=%async_computation | async-start | bytes 131072 | tf_op jit(solution)/shard_map/all_to_all | solution.py:121
  197.5 11.7 %all-to-all-start.1 = ((f32[1,4,128,128]{3,1,0,2:T(4,128)}), f32[1,4,128,128]{3,1,0,2:T(4,128)S(1)}, u32[]{:S(2)}, u32[]{:S(2)}) async-start(f32[1,4,128,128]{3,1,0,2:T(4,128)} %bitcast.111), calls=%async_computation.1 | async-start | bytes 524288 | tf_op jit(solution)/shard_map/all_to_all | solution.py:120
  201.1 8.1 %copy-start.4 = (f32[4,16,128]{2,1,0:T(8,128)S(1)}, f32[4,16,128]{2,1,0:T(8,128)}, u32[]{:S(2)}) copy-start(f32[4,16,128]{2,1,0:T(8,128)} %param.34) | copy-start | bytes 98308
  214.9 12.9 %all-to-all-start.2 = ((f32[8,4,16,128]{3,2,1,0:T(8,128)}), f32[8,4,16,128]{3,2,1,0:T(8,128)S(1)}, u32[]{:S(2)}, u32[]{:S(2)}) async-start(f32[8,4,16,128]{3,2,1,0:T(8,128)} %get-tuple-element.85), calls=%async_computation.2 | async-start | bytes 524288 | tf_op jit(solution)/shard_map/all_to_all | solution.py:131
  218.3 100.2 %reduce-scatter.2.cloned.1.call-start = ((), (), s32[]{:S(2)}) async-start(), calls=%async_computation.5 | async-start | bytes 7864320 | tf_op jit(solution)/shard_map/reduce_scatter | solution.py:149
  222.8 1.1 copy-start.7
  223.9 23.8 %collective-permute-start = (f32[2,512]{1,0:T(2,128)S(1)}, f32[2,512]{1,0:T(2,128)S(1)}, u32[]{:S(2)}, u32[]{:S(2)}) collective-permute-start(f32[2,512]{1,0:T(2,128)S(1)} %slice.29), channel_id=1, source_target_pairs={{0,4},{4,8},{8,12},{12,16},{16,20},{20,24},{24,28},{1,5},{5,9},{9,... | collective-permute-start | bytes 12296 | tf_op jit(solution)/shard_map/ppermute | solution.py:19
  260.4 0.7 copy-start.6
  318.5 1.9 copy-start.1
Sparse Core Ops, SparseCore 0:
  8.9 31.2 all-gather.1
  260.6 57.9 reduce-scatter.1
where the time goes:
time: 330 us; the launch traced here: 328 us
  matrix products  127 us (38%)
  waiting for transfers between devices  97.7 us (30%)
  local copies, waits for them, and re-layouts  43.7 us (13%)
  other arithmetic  29.4 us (9%)
  starting transfers between devices  16.4 us (5%)
  between operations  13.6 us (4%)
    reduce_scatter x1, waiting for transfers between devices, shards(): lax.psum_scatter(jnp.dot(rec_out, recurrence_output_weight, preferred_ele...  57.4 us
    all_gather x1, waiting for transfers between devices, shards(): collected_rows = lax.all_gather(layer_input, 'tp', axis=1, tiled=True)  30 us
    dot_general x5, matrix products, shards(): jnp.dot(normed, weight, preferred_element_type=jnp.float32)  27.2 us
    dot_general x12, matrix products, block_pass(): jnp.einsum('bqy,byx->bqx', query_scaled_rows, latent_state, precision=PRE...  23.4 us
    dot_general x12, matrix products, block_pass(): jnp.einsum('otm,ote->ome', scaled_key * jnp.exp(block_total)[:, None, :],...  19.4 us
    dynamic_update_slice x12, other arithmetic, shards(): lax.scan(block_pass, (zero_state, zero_total), (to_blocks(query_rows, DK)...  19.2 us
    dot_general x12, matrix products, block_pass(): jnp.einsum('htk,hsk->hts', query_scaled_rows, scaled_key, precision=PRECI...  15.9 us
    dot_general x12, matrix products, block_pass(): jnp.einsum('hts,hsv->htv', scores, value_rows, precision=PRECISE_PRODUCT)  14 us
  transfers between devices with their start and end apart: 6, of which 4 were waited for; matrix products, arithmetic and copies ran while one was open for 10% of the time, Pallas kernels for 0%

commit v1 on v0

v1 whole, which is shorter than its diff:
```python
import functools

import jax
import jax.numpy as jnp
from jax import lax
from jax.experimental import pallas as pl
from jax.experimental.pallas import tpu as pltpu
from jax.sharding import PartitionSpec as P

DK = 128
DV = 128
CK = 3
BLK = 64
ROWS = 128


EPS = 1e-06
F32 = jnp.float32
BF16 = jnp.bfloat16


def from_behind(value, axis, by):
    peers = lax.axis_size(axis)
    pairs = [(i, i + by) for i in range(peers) if 0 <= i + by < peers]
    return lax.ppermute(value, axis, pairs)


def rms_scale(value_rows):
    return lax.rsqrt(jnp.mean(value_rows * value_rows, axis=-1, keepdims=True) + EPS)


def nt_dot(a, b):
    return lax.dot_general(a, b, (((1,), (1,)), ((), ())), preferred_element_type=F32)


def tn_dot(a, b):
    return lax.dot_general(a, b, (((0,), (0,)), ((), ())), preferred_element_type=F32)


def local_kernel(
    heads, q_ref, f_ref, v_ref, surge_ref, fmin_ref, part_ref, shift_ref, state_ref, total_ref, st, run
):
    step = pl.program_id(0)

    @pl.when(step == 0)
    def _():
        st[...] = jnp.zeros_like(st)
        run[...] = jnp.zeros_like(run)

    row = lax.broadcasted_iota(jnp.int32, (BLK, BLK), 0)
    col = lax.broadcasted_iota(jnp.int32, (BLK, BLK), 1)
    causal = col <= row
    middle = (causal.astype(F32) - (col < BLK // 2).astype(F32))
    for b in range(q_ref.shape[0] // BLK):
        rows = slice(b * BLK, (b + 1) * BLK)
        forget = f_ref[rows, :].astype(F32)
        keys = (1.0 - fmin_ref[...]) * jax.nn.sigmoid(-forget)
        logs = jnp.log1p(-keys) + surge_ref[rows, :]
        rel = jnp.dot(middle, logs, precision=lax.Precision.HIGHEST, preferred_element_type=F32)
        mid = logs[0:1, :] - rel[0:1, :]
        tail = rel[BLK - 1 : BLK, :]
        raw = q_ref[rows, :].astype(F32)
        queries = raw * jax.nn.sigmoid(raw) * DK ** (-0.5)
        q_mid = queries * jnp.exp(rel)
        k_mid = keys * jnp.exp(-rel)
        q_in = q_mid * jnp.exp(mid)
        k_out = (k_mid * jnp.exp(tail)).astype(BF16)
        whole = jnp.exp(mid + tail)
        shift_ref[rows, :] = (q_in * jnp.exp(run[...])).astype(BF16)
        run[...] = run[...] + mid + tail
        q_mid = q_mid.astype(BF16)
        k_mid = k_mid.astype(BF16)
        q_in = q_in.astype(BF16)
        values = v_ref[rows, :]
        for h in range(heads):
            ch = slice(h * DK, (h + 1) * DK)
            scores = jnp.where(causal, nt_dot(q_mid[:, ch], k_mid[:, ch]), 0.0).astype(BF16)
            before = st[h]
            part_ref[rows, ch] = jnp.dot(
                scores, values[:, ch], preferred_element_type=F32
            ) + nt_dot(q_in[:, ch], before.astype(BF16))
            st[h] = before * whole[:, ch] + tn_dot(values[:, ch], k_out[:, ch])

    @pl.when(step == pl.num_programs(0) - 1)
    def _():
        for h in range(heads):
            state_ref[h] = st[h].T
        total_ref[...] = run[...]


def local_pass(query_raw, forget_raw, value_raw, surge, fmin):
    tokens, width = query_raw.shape
    heads = width // DK
    rows = ROWS if tokens % ROWS == 0 else BLK
    tile = pl.BlockSpec((rows, width), lambda i: (i, 0))
    line = pl.BlockSpec((1, width), lambda i: (0, 0))
    return pl.pallas_call(
        functools.partial(local_kernel, heads),
        grid=(tokens // rows,),
        in_specs=[tile, tile, tile, tile, line],
        out_specs=[
            tile,
            tile,
            pl.BlockSpec((heads, DK, DV), lambda i: (0, 0, 0)),
            line,
        ],
        out_shape=[
            jax.ShapeDtypeStruct((tokens, width), F32),
            jax.ShapeDtypeStruct((tokens, width), BF16),
            jax.ShapeDtypeStruct((heads, DK, DV), F32),
            jax.ShapeDtypeStruct((1, width), F32),
        ],
        scratch_shapes=[pltpu.VMEM((heads, DV, DK), F32), pltpu.VMEM((1, width), F32)],
        cost_estimate=pl.CostEstimate(
            flops=tokens * width * 1000, bytes_accessed=tokens * width * 16, transcendentals=0
        ),
        name="local_pass",
    )(query_raw, forget_raw, value_raw, surge, fmin)


def shards(
    layer_input,
    input_norm_gain,
    query_weight,
    forget_weight,
    value_matrix,
    output_gate_weight,
    after_gate_weight,
    before_gate_weight,
    convolution_input_weight,
    forget_minimum,
    surge_log_decay,
    convolution_kernel,
    head_norm_gain,
    starting_state,
    recurrence_output_weight,
    convolution_output_weight,
    output_norm_gain,
):
    tokens_dev = layer_input.shape[0]
    heads_local = query_weight.shape[1] // DK
    weight_list = (
        query_weight,
        forget_weight,
        value_matrix,
        output_gate_weight,
        after_gate_weight,
        before_gate_weight,
        convolution_input_weight,
    )
    collected_rows = lax.all_gather(layer_input, "tp", axis=1, tiled=True)
    rows_f = collected_rows.astype(jnp.float32)
    normed = (rows_f * rms_scale(rows_f) * input_norm_gain.astype(jnp.float32)).astype(jnp.bfloat16)
    projections = tuple(
        (
            jnp.dot(normed, weight, preferred_element_type=jnp.float32).astype(jnp.bfloat16)
            for weight in weight_list
        )
    )
    query_raw, forget_raw, value_raw, outgate_raw, postgate_raw, pregate_raw, convval_raw = (
        projections
    )
    partial_output, shifted_query, local_state, local_total = local_pass(
        query_raw, forget_raw, value_raw, surge_log_decay, forget_minimum[None, :]
    )
    local_total = local_total.reshape(heads_local, DK)
    moved_state, moved_total = (
        lax.all_to_all(local_state[None], "sp", split_axis=2, concat_axis=0, tiled=True),
        lax.all_to_all(
            local_total[None, :, :, None], "sp", split_axis=2, concat_axis=0, tiled=True
        ),
    )
    running = starting_state
    entering = []
    for i in range(moved_state.shape[0]):
        entering.append(running)
        running = jnp.exp(moved_total[i]) * running + moved_state[i]
    carried_state = lax.all_to_all(
        jnp.stack(entering), "sp", split_axis=0, concat_axis=2, tiled=True
    )[0].astype(BF16)
    recurrence_step = partial_output.reshape(tokens_dev, heads_local, DV) + jnp.einsum(
        "xoq,oqu->xou",
        shifted_query.reshape(tokens_dev, heads_local, DK),
        carried_state,
        preferred_element_type=F32,
    )
    normed_heads = recurrence_step * rms_scale(recurrence_step) * head_norm_gain.astype(jnp.float32)
    rec_out = (
        normed_heads.reshape(tokens_dev, heads_local * DV)
        * jax.nn.silu(outgate_raw.astype(jnp.float32))
    ).astype(jnp.bfloat16)
    mixed_in = pregate_raw.astype(jnp.float32) * convval_raw.astype(jnp.float32)
    rim_rows = from_behind(mixed_in[tokens_dev - (CK - 1) :], "sp", 1)
    padded = jnp.concatenate([rim_rows, mixed_in], axis=0)
    taps_f = convolution_kernel.astype(jnp.float32)
    conv_sum = padded[0:tokens_dev] * taps_f[0]
    for offset in range(1, CK):
        conv_sum = conv_sum + padded[offset : offset + tokens_dev] * taps_f[offset]
    conv_out = (postgate_raw.astype(jnp.float32) * conv_sum).astype(jnp.bfloat16)
    mixed = lax.psum_scatter(
        (
            jnp.dot(rec_out, recurrence_output_weight, preferred_element_type=jnp.float32)
            + jnp.dot(conv_out, convolution_output_weight, preferred_element_type=jnp.float32)
        ).astype(BF16),
        "tp",
        scatter_dimension=0,
        tiled=True,
    ).astype(F32)
    return (mixed * rms_scale(mixed) * output_norm_gain.astype(jnp.float32)).astype(jnp.bfloat16)


def solution(mesh):
    return jax.shard_map(
        shards,
        mesh=mesh,
        in_specs=(
            P("sp", "tp"),
            P(),
            P(None, "tp"),
            P(None, "tp"),
            P(None, "tp"),
            P(None, "tp"),
            P(None, "tp"),
            P(None, "tp"),
            P(None, "tp"),
            P("tp"),
            P("sp", "tp"),
            P(None, "tp"),
            P(),
            P("tp", "sp", None),
            P("tp", None),
            P("tp", None),
            P(),
        ),
        out_specs=P(("sp", "tp"), None),
        check_vma=False,
    )
```

time: 330 us -> 186 us (0.56)
  matrix products: 127 us -> 43.8 us
  local copies, waits for them, and re-layouts: 43.7 us -> 12.4 us
  waiting for transfers between devices: 97.7 us -> 75.8 us
  other arithmetic: 29.4 us -> 13.2 us
  Pallas kernels: 0 us -> 9.96 us
    dot_general x49 -> x1, matrix products: 77.1 us -> 1.85 us  [shards(): jnp.einsum('xoq,oqu->xou', shifted_query.reshape(tokens_dev, heads_local,...]
    reduce_scatter x1, waiting for transfers between devices: 57.4 us -> 36.4 us  [shards(): lax.psum_scatter((jnp.dot(rec_out, recurrence_output_weight, preferred_el...]
    dynamic_update_slice x12 -> x0, other arithmetic: 19.2 us -> none  [shards(): lax.scan(block_pass, (zero_state, zero_total), (to_blocks(query_rows, DK)...]
    transpose x4 -> x0, local copies, waits for them, and re-layouts: 12.7 us -> none  [the longest x3 9.04 us: to_blocks(): value_rows.reshape(blocks, BLK, heads_local, width).transpose(0, 2, 1, 3)]
    squeeze x12 -> x0, local copies, waits for them, and re-layouts: 11 us -> none  [shards(): lax.scan(block_pass, (zero_state, zero_total), (to_blocks(query_rows, DK)...]
    pallas_call x0 -> x1, Pallas kernels: none -> 9.96 us  [local_pass(): pl.pallas_call(functools.partial(local_kernel, heads), grid=(tokens // ro...]
    dot_general x5, matrix products: 27.2 us -> 20.9 us  [shards(): jnp.dot(normed, weight, preferred_element_type=jnp.float32)]
    dynamic_update_slice x8 -> x0, local copies, waits for them, and re-layouts: 5 us -> none  [shards(): _, entering = lax.scan(advance, starting_state, (moved_state, moved_total))]
  transfers between devices with their start and end apart: 6 -> 6, of which waited for: 4 -> 4; matrix products, arithmetic and copies ran while one was open for 10% -> 19% of each run, Pallas kernels for 0% -> 0%
where the time goes in v1:
time: 186 us; the launch traced here: 185 us
  waiting for transfers between devices  75.8 us (41%)
  matrix products  43.8 us (24%)
  starting transfers between devices  16.4 us (9%)
  between operations  13.5 us (7%)
  other arithmetic  13.2 us (7%)
  local copies, waits for them, and re-layouts  12.4 us (7%)
  Pallas kernels  9.96 us (5%)
    reduce_scatter x1, waiting for transfers between devices, shards(): lax.psum_scatter((jnp.dot(rec_out, recurrence_output_weight, preferred_el...  36.4 us
    all_gather x1, waiting for transfers between devices, shards(): collected_rows = lax.all_gather(layer_input, 'tp', axis=1, tiled=True)  30.8 us
    dot_general x5, matrix products, shards(): jnp.dot(normed, weight, preferred_element_type=jnp.float32)  20.9 us
    dot_general x1, matrix products, shards(): jnp.dot(conv_out, convolution_output_weight, preferred_element_type=jnp.f...  11.7 us
    pallas_call x1, Pallas kernels, local_pass(): pl.pallas_call(functools.partial(local_kernel, heads), grid=(tokens // ro...  9.96 us
    dot_general x1, matrix products, shards(): jnp.dot(rec_out, recurrence_output_weight, preferred_element_type=jnp.flo...  9.28 us
    all_to_all x1, starting transfers between devices, shards(): lax.all_to_all(local_total[None, :, :, None], 'sp', split_axis=2, concat_...  5.52 us
    all_to_all x1, waiting for transfers between devices, shards(): lax.all_to_all(local_total[None, :, :, None], 'sp', split_axis=2, concat_...  5.03 us
  transfers between devices with their start and end apart: 6, of which 4 were waited for; matrix products, arithmetic and copies ran while one was open for 19% of the time, Pallas kernels for 0%

profile of v1, /device:TPU:0, one launch (start us, length us, event | category | flops | bytes accessed | tf_op | source)
XLA Modules:
  0.0 185.1 jit_solution(9842480239257165601)
XLA Ops:
  6.5 0.7 all-gather.2.cloned.1.call-update
  7.3 0.7 convert_element_type.79
  7.9 1.4 bitcast_dynamic-update-slice_fusion.6
  9.3 30.8 %all-gather.2.cloned.1.call-done = bf16[768,2048]{1,0:T(8,128)(2,1)} async-done(((bf16[768,512]{1,0:T(8,128)(2,1)}), bf16[768,2048]{1,0:T(8,128)(2,1)}) %all-gather.2.cloned.1.call-update) | async-done | bytes 3145744 | tf_op jit(solution)/shard_map/all_gather | solution.py:151
  40.2 2.7 %fusion = f32[768]{0:T(1024)S(1)} fusion(bf16[768,2048]{1,0:T(8,128)(2,1)} %all-gather.2.cloned.1.call-done), kind=kLoop, calls=%fused_computation.2 | loop fusion | flops 4717824 | bytes 3148800 | tf_op jit(solution)/shard_map/reduce_sum | solution.py:29
  43.0 4.5 %convolution_convert_fusion.4.v_ref = bf16[768,512]{1,0:T(8,128)(2,1)} fusion(bf16[2048,512]{1,0:T(8,128)(2,1)} %param.21, bf16[768,2048]{1,0:T(8,128)(2,1)S(1)} %copy-done.1, f32[2048]{0:T(1024)S(1)} %convert_element_type.79, f32[768]{0:T(1024)S(1)} %add_rsqrt_fusion.1), kind=kOutput, calls=%fused_computation.36 | convolution fusion | flops 1617297408 | bytes 6040576 | tf_op jit(solution)/shard_map/dot_general | solution.py:156
  47.5 2.7 %convolution_convert_fusion.5.f_ref = bf16[768,512]{1,0:T(8,128)(2,1)} fusion(bf16[2048,512]{1,0:T(8,128)(2,1)S(1)} %copy-done.6, bf16[768,2048]{1,0:T(8,128)(2,1)S(1)} %copy-done.1, f32[2048]{0:T(1024)S(1)} %convert_element_type.79, f32[768]{0:T(1024)S(1)} %add_rsqrt_fusion.1), kind=kOutput, calls=%fused_computation.37 | convolution fusion | flops 1617297408 | bytes 6040576 | tf_op jit(solution)/shard_map/dot_general | solution.py:156
  50.2 2.7 %convolution_convert_fusion.6.q_ref = bf16[768,512]{1,0:T(8,128)(2,1)} fusion(bf16[2048,512]{1,0:T(8,128)(2,1)S(1)} %copy-done.7, bf16[768,2048]{1,0:T(8,128)(2,1)S(1)} %copy-done.1, f32[2048]{0:T(1024)S(1)} %convert_element_type.79, f32[768]{0:T(1024)S(1)} %add_rsqrt_fusion.1), kind=kOutput, calls=%fused_computation.38 | convolution fusion | flops 1617297408 | bytes 6040576 | tf_op jit(solution)/shard_map/dot_general | solution.py:156
  52.9 10.0 %local_pass.1 = (f32[768,512]{1,0:T(8,128)}, bf16[768,512]{1,0:T(8,128)(2,1)}, f32[4,128,128]{2,1,0:T(8,128)}, f32[1,512]{1,0:T(1,128)}) custom-call(bf16[768,512]{1,0:T(8,128)(2,1)} %convolution_convert_fusion.6.q_ref, bf16[768,512]{1,0:T(8,128)(2,1)} %convolution_convert_fusion.5.f_ref, bf16[768,512]{1,0:T(8,128)(2,1)} %convolution_convert_fusion.4.v_ref, ...), custom_call_target="tpu_custom_call" | custom-call | flops 393216000 | bytes 6291456 | tf_op jit(solution)/shard_map/local_pass/pallas_call | solution.py:97
  62.9 1.4 copy.34
  64.3 5.5 %all-to-all-start = ((f32[1,4,128,1]{1,3,0,2:T(1,128)}), f32[1,4,128,1]{1,3,0,2:T(1,128)S(1)}, u32[]{:S(2)}, u32[]{:S(2)}) async-start(f32[1,4,128,1]{1,3,0,2:T(1,128)} %copy.34), calls=%async_computation | async-start | bytes 131072 | tf_op jit(solution)/shard_map/all_to_all | solution.py:169
  69.9 1.8 copy.36
  71.7 5.0 %all-to-all-done = f32[1,4,128,1]{1,3,0,2:T(1,128)S(1)} async-done(((f32[1,4,128,1]{1,3,0,2:T(1,128)}), f32[1,4,128,1]{1,3,0,2:T(1,128)S(1)}, u32[]{:S(2)}, u32[]{:S(2)}) %all-to-all-start) | async-done | bytes 2080 | tf_op jit(solution)/shard_map/all_to_all | solution.py:169
  76.8 3.4 %all-to-all-start.1 = ((f32[1,4,128,128]{3,1,0,2:T(4,128)}), f32[1,4,128,128]{3,1,0,2:T(4,128)S(1)}, u32[]{:S(2)}, u32[]{:S(2)}) async-start(f32[1,4,128,128]{3,1,0,2:T(4,128)} %copy.36), calls=%async_computation.1 | async-start | bytes 524288 | tf_op jit(solution)/shard_map/all_to_all | solution.py:168
  80.2 5.3 %convolution_convert_fusion = bf16[768,512]{1,0:T(8,128)(2,1)} fusion(bf16[2048,512]{1,0:T(8,128)(2,1)} %param.25, bf16[768,2048]{1,0:T(8,128)(2,1)} %all-gather.2.cloned.1.call-done, f32[2048]{0:T(1024)S(1)} %convert_element_type.79, f32[768]{0:T(1024)S(1)} %add_rsqrt_fusion.1), kind=kOutput, calls=%fused_computation.32 | convolution fusion | flops 1617297408 | bytes 6040576 | tf_op jit(solution)/shard_map/dot_general | solution.py:156
  85.6 2.8 %all-to-all-done.1 = f32[1,4,128,128]{3,1,0,2:T(4,128)S(1)} async-done(((f32[1,4,128,128]{3,1,0,2:T(4,128)}), f32[1,4,128,128]{3,1,0,2:T(4,128)S(1)}, u32[]{:S(2)}, u32[]{:S(2)}) %all-to-all-start.1) | async-done | bytes 262176 | tf_op jit(solution)/shard_map/all_to_all | solution.py:168
  89.1 0.7 bitcast_dynamic-update-slice_fusion.4
  90.5 0.7 bitcast_dynamic-update-slice_fusion.2
  91.9 0.7 bitcast_dynamic-update-slice_fusion
  93.2 3.4 %all-to-all-start.2 = ((bf16[8,4,16,128]{3,2,1,0:T(8,128)(2,1)}), bf16[8,4,16,128]{3,2,1,0:T(8,128)(2,1)S(1)}, u32[]{:S(2)}, u32[]{:S(2)}) async-start(bf16[8,4,16,128]{3,2,1,0:T(8,128)(2,1)} %fusion.24), calls=%async_computation.2 | async-start | bytes 262144 | tf_op jit(solution)/shard_map/all_to_all | solution.py:178
  96.7 5.7 %convert_multiply_fusion.5 = f32[768,512]{1,0:T(8,128)} fusion(bf16[768,512]{1,0:T(8,128)(2,1)} %convolution_convert_fusion, bf16[2048,512]{1,0:T(8,128)(2,1)} %param.24, bf16[768,2048]{1,0:T(8,128)(2,1)} %all-gather.2.cloned.1.call-done, f32[2048]{0:T(1024)S(1)} %convert_element_type.79, f32[768]{0:T(1024)S(1)} %add_rsqrt_fusion.1), kind=kOutput, calls=%fused_computation.28 | convolution fusion | flops 1618477056 | bytes 7613440 | tf_op jit(solution)/shard_map/dot_general | solution.py:156
  102.4 3.1 %copy.44 = f32[768,512]{0,1:T(8,128)} copy(f32[768,512]{1,0:T(8,128)} %get-tuple-element.9) | data formatting | bytes 3145728 | tf_op jit(solution)/shard_map/reshape | solution.py:181
  105.5 0.7 slice.108
  106.2 4.1 %collective-permute-start = (f32[2,512]{1,0:T(2,128)S(1)}, f32[2,512]{1,0:T(2,128)S(1)}, u32[]{:S(2)}, u32[]{:S(2)}) collective-permute-start(f32[2,512]{1,0:T(2,128)S(1)} %slice.108), channel_id=1, source_target_pairs={{0,4},{4,8},{8,12},{12,16},{16,20},{20,24},{24,28},{1,5},{5,9},{9,... | collective-permute-start | bytes 12296 | tf_op jit(solution)/shard_map/ppermute | solution.py:25
  110.3 1.8 multiply_reduce_fusion
  112.2 1.4 multiply_multiply_fusion
  113.6 3.0 %copy.42 = f32[768,512]{1,0:T(8,128)} copy(f32[768,512]{0,1:T(8,128)} %bitcast.116) | data formatting | bytes 3145728 | tf_op jit(solution)/shard_map/reshape | solution.py:189
  116.6 9.3 %fusion.18 = f32[768,2048]{1,0:T(8,128)} fusion(bf16[512,2048]{1,0:T(8,128)(2,1)S(1)} %copy-done, f32[768,512]{1,0:T(8,128)} %copy.42, bf16[2048,512]{1,0:T(8,128)(2,1)} %param.22, bf16[768,2048]{1,0:T(8,128)(2,1)} %all-gather.2.cloned.1.call-done, f32[2048]{0:T(1024)S(1)} %convert_element_type.79, f32[768]{0:T(1024)S(1)} %add_rsqrt_fusion.1), kind=kOutput, calls=%fused_computation.39 | convolution fusion | flops 3230662656 | bytes 15215616 | tf_op jit(solution)/shard_map/dot_general | solution.py:202
  125.9 11.7 %add_convert_fusion = bf16[768,2048]{1,0:T(8,128)(2,1)} fusion(f32[768,2048]{1,0:T(8,128)} %fusion.18, bf16[512,2048]{1,0:T(8,128)(2,1)} %param.32, f32[2,512]{1,0:T(2,128)S(1)} %collective-permute-done, f32[768,512]{1,0:T(8,128)} %convert_multiply_fusion.5, bf16[2048,512]{1,0:T(8,128)(2,1)} %param.23, f32[512]{0:T(512)S(1)} %bitcast.143, ...), kind=kOutput, calls=%fused_computation.5 | convolution fusion | flops 3234988032 | bytes 18371584 | tf_op jit(solution)/shard_map/dot_general | solution.py:203
  138.3 36.4 %reduce-scatter.2.cloned.1.call-done = bf16[192,2048]{1,0:T(8,128)(2,1)} async-done(((bf16[768,2048]{1,0:T(8,128)(2,1)}), bf16[192,2048]{1,0:T(8,128)(2,1)}) %reduce-scatter.2.cloned.1.call-update) | async-done | bytes 786448 | tf_op jit(solution)/shard_map/reduce_scatter | solution.py:200
  174.6 1.4 fusion.13
  176.0 2.3 %fusion.15 = bf16[192,2048]{1,0:T(8,128)(2,1)} fusion(bf16[192,2048]{1,0:T(8,128)(2,1)} %reduce-scatter.2.cloned.1.call-done, f32[2048]{0:T(1024)S(1)} %convert_element_type.102, f32[192]{0:T(256)S(1)} %add_rsqrt_fusion.2), kind=kLoop, calls=%fused_computation.24 | loop fusion | flops 1572864 | bytes 1581824 | tf_op jit(solution)/shard_map/convert_element_type | solution.py:209
  (37 shorter events, 3.8 us)
Async XLA Ops:
  6.5 110.0 %copy-start = (bf16[512,2048]{1,0:T(8,128)(2,1)S(1)}, bf16[512,2048]{1,0:T(8,128)(2,1)}, u32[]{:S(2)}) copy-start(bf16[512,2048]{1,0:T(8,128)(2,1)} %param.31) | copy-start | bytes 6291460
  6.5 33.6 %all-gather.2.cloned.1.call-start = ((), (), s32[]{:S(2)}) async-start(), calls=%async_computation.4 | async-start | bytes 3932160 | tf_op jit(solution)/shard_map/all_gather | solution.py:151
  40.2 2.8 %copy-start.1 = (bf16[768,2048]{1,0:T(8,128)(2,1)S(1)}, bf16[768,2048]{1,0:T(8,128)(2,1)}, u32[]{:S(2)}) copy-start(bf16[768,2048]{1,0:T(8,128)(2,1)} %all-gather.2.cloned.1.call-done) | copy-start | bytes 9437188
  43.0 4.5 %copy-start.6 = (bf16[2048,512]{1,0:T(8,128)(2,1)S(1)}, bf16[2048,512]{1,0:T(8,128)(2,1)}, u32[]{:S(2)}) copy-start(bf16[2048,512]{1,0:T(8,128)(2,1)} %param.20) | copy-start | bytes 6291460
  47.5 2.7 %copy-start.7 = (bf16[2048,512]{1,0:T(8,128)(2,1)S(1)}, bf16[2048,512]{1,0:T(8,128)(2,1)}, u32[]{:S(2)}) copy-start(bf16[2048,512]{1,0:T(8,128)(2,1)} %param.19) | copy-start | bytes 6291460
  52.9 16.9 %copy-start.4 = (bf16[3,512]{1,0:T(4,128)(2,1)S(1)}, bf16[3,512]{1,0:T(4,128)(2,1)}, u32[]{:S(2)}) copy-start(bf16[3,512]{1,0:T(4,128)(2,1)} %param.28) | copy-start | bytes 9220
  52.9 16.9 %copy-start.8 = (bf16[128]{0:T(256)(128)(2,1)S(1)}, bf16[128]{0:T(256)(128)(2,1)}, u32[]{:S(2)}) copy-start(bf16[128]{0:T(256)(128)(2,1)} %param.29) | copy-start | bytes 772
  64.3 12.4 %all-to-all-start = ((f32[1,4,128,1]{1,3,0,2:T(1,128)}), f32[1,4,128,1]{1,3,0,2:T(1,128)S(1)}, u32[]{:S(2)}, u32[]{:S(2)}) async-start(f32[1,4,128,1]{1,3,0,2:T(1,128)} %copy.34), calls=%async_computation | async-start | bytes 131072 | tf_op jit(solution)/shard_map/all_to_all | solution.py:169
  76.8 11.7 %all-to-all-start.1 = ((f32[1,4,128,128]{3,1,0,2:T(4,128)}), f32[1,4,128,128]{3,1,0,2:T(4,128)S(1)}, u32[]{:S(2)}, u32[]{:S(2)}) async-start(f32[1,4,128,128]{3,1,0,2:T(4,128)} %copy.36), calls=%async_computation.1 | async-start | bytes 524288 | tf_op jit(solution)/shard_map/all_to_all | solution.py:168
  80.2 8.3 %copy-start.3 = (f32[4,16,128]{2,1,0:T(8,128)S(1)}, f32[4,16,128]{2,1,0:T(8,128)}, u32[]{:S(2)}) copy-start(f32[4,16,128]{2,1,0:T(8,128)} %param.30) | copy-start | bytes 98308
  93.2 17.0 %all-to-all-start.2 = ((bf16[8,4,16,128]{3,2,1,0:T(8,128)(2,1)}), bf16[8,4,16,128]{3,2,1,0:T(8,128)(2,1)S(1)}, u32[]{:S(2)}, u32[]{:S(2)}) async-start(bf16[8,4,16,128]{3,2,1,0:T(8,128)(2,1)} %fusion.24), calls=%async_computation.2 | async-start | bytes 262144 | tf_op jit(solution)/shard_map/all_to_all | solution.py:178
  96.6 78.0 %reduce-scatter.2.cloned.1.call-start = ((), (), s32[]{:S(2)}) async-start(), calls=%async_computation.5 | async-start | bytes 3932160 | tf_op jit(solution)/shard_map/reduce_scatter | solution.py:200
  102.4 7.9 %copy-start.2 = (bf16[768,512]{1,0:T(8,128)(2,1)S(1)}, bf16[768,512]{1,0:T(8,128)(2,1)}, u32[]{:S(2)}) copy-start(bf16[768,512]{1,0:T(8,128)(2,1)} %get-tuple-element.12) | copy-start | bytes 2359300
  106.2 19.7 %collective-permute-start = (f32[2,512]{1,0:T(2,128)S(1)}, f32[2,512]{1,0:T(2,128)S(1)}, u32[]{:S(2)}, u32[]{:S(2)}) collective-permute-start(f32[2,512]{1,0:T(2,128)S(1)} %slice.108), channel_id=1, source_target_pairs={{0,4},{4,8},{8,12},{12,16},{16,20},{20,24},{24,28},{1,5},{5,9},{9,... | collective-permute-start | bytes 12296 | tf_op jit(solution)/shard_map/ppermute | solution.py:25
  137.6 0.7 copy-start.5
Sparse Core Ops, SparseCore 0:
  8.9 31.2 all-gather.1
  137.7 36.8 reduce-scatter.1

commit v2 on v1

v2 whole, which is shorter than its diff:
```python
import functools

import jax
import jax.numpy as jnp
from jax import lax
from jax.experimental import pallas as pl
from jax.experimental.pallas import tpu as pltpu
from jax.sharding import PartitionSpec as P

DK = 128
DV = 128
CK = 3
BLK = 64
ROWS = 128


EPS = 1e-06
F32 = jnp.float32
BF16 = jnp.bfloat16
MESH = pl.DeviceIdType.MESH


def rms_scale(value_rows):
    return lax.rsqrt(jnp.mean(value_rows * value_rows, axis=-1, keepdims=True) + EPS)


def nt_dot(a, b):
    return lax.dot_general(a, b, (((1,), (1,)), ((), ())), preferred_element_type=F32)


def tn_dot(a, b):
    return lax.dot_general(a, b, (((0,), (0,)), ((), ())), preferred_element_type=F32)


def local_kernel(
    heads, q_ref, f_ref, v_ref, surge_ref, fmin_ref, part_ref, shift_ref, pack_ref, st, run
):
    step = pl.program_id(0)

    @pl.when(step == 0)
    def _():
        st[...] = jnp.zeros_like(st)
        run[...] = jnp.zeros_like(run)

    row = lax.broadcasted_iota(jnp.int32, (BLK, BLK), 0)
    col = lax.broadcasted_iota(jnp.int32, (BLK, BLK), 1)
    causal = col <= row
    middle = (causal.astype(F32) - (col < BLK // 2).astype(F32))
    for b in range(q_ref.shape[0] // BLK):
        rows = slice(b * BLK, (b + 1) * BLK)
        forget = f_ref[rows, :].astype(F32)
        keys = (1.0 - fmin_ref[...]) * jax.nn.sigmoid(-forget)
        logs = jnp.log1p(-keys) + surge_ref[rows, :]
        rel = jnp.dot(middle, logs, precision=lax.Precision.HIGHEST, preferred_element_type=F32)
        mid = logs[0:1, :] - rel[0:1, :]
        tail = rel[BLK - 1 : BLK, :]
        raw = q_ref[rows, :].astype(F32)
        queries = raw * jax.nn.sigmoid(raw) * DK ** (-0.5)
        q_mid = queries * jnp.exp(rel)
        k_mid = keys * jnp.exp(-rel)
        q_in = q_mid * jnp.exp(mid)
        k_out = (k_mid * jnp.exp(tail)).astype(BF16)
        whole = jnp.exp(mid + tail)
        shift_ref[rows, :] = (q_in * jnp.exp(run[...])).astype(BF16)
        run[...] = run[...] + mid + tail
        q_mid = q_mid.astype(BF16)
        k_mid = k_mid.astype(BF16)
        q_in = q_in.astype(BF16)
        values = v_ref[rows, :]
        for h in range(heads):
            ch = slice(h * DK, (h + 1) * DK)
            scores = jnp.where(causal, nt_dot(q_mid[:, ch], k_mid[:, ch]), 0.0).astype(BF16)
            before = st[h]
            part_ref[rows, ch] = jnp.dot(
                scores, values[:, ch], preferred_element_type=F32
            ) + nt_dot(q_in[:, ch], before.astype(BF16))
            st[h] = before * whole[:, ch] + tn_dot(values[:, ch], k_out[:, ch])

    @pl.when(step == pl.num_programs(0) - 1)
    def _():
        peers, _, piece, _ = pack_ref.shape
        lane = lax.broadcasted_iota(jnp.int32, (DK, DV), 1)
        whole = jnp.exp(run[...])
        decays = jnp.zeros((DK, DV), F32)
        for h in range(heads):
            ch = slice(h * DK, (h + 1) * DK)
            state = st[h].T
            decays = jnp.where(lane == h, jnp.broadcast_to(whole[:, ch], (DV, DK)).T, decays)
            for p in range(peers):
                pack_ref[p, h] = state[p * piece : (p + 1) * piece]
        for p in range(peers):
            pack_ref[p, heads] = decays[p * piece : (p + 1) * piece]


def local_pass(peers, query_raw, forget_raw, value_raw, surge, fmin):
    tokens, width = query_raw.shape
    heads = width // DK
    rows = ROWS if tokens % ROWS == 0 else BLK
    tile = pl.BlockSpec((rows, width), lambda i: (i, 0))
    line = pl.BlockSpec((1, width), lambda i: (0, 0))
    return pl.pallas_call(
        functools.partial(local_kernel, heads),
        grid=(tokens // rows,),
        in_specs=[tile, tile, tile, tile, line],
        out_specs=[
            tile,
            tile,
            pl.BlockSpec((peers, heads + 1, DK // peers, DV), lambda i: (0, 0, 0, 0)),
        ],
        out_shape=[
            jax.ShapeDtypeStruct((tokens, width), F32),
            jax.ShapeDtypeStruct((tokens, width), BF16),
            jax.ShapeDtypeStruct((peers, heads + 1, DK // peers, DV), F32),
        ],
        scratch_shapes=[pltpu.VMEM((heads, DV, DK), F32), pltpu.VMEM((1, width), F32)],
        cost_estimate=pl.CostEstimate(
            flops=tokens * width * 1000, bytes_accessed=tokens * width * 16, transcendentals=0
        ),
        name="local_pass",
    )(query_raw, forget_raw, value_raw, surge, fmin)


def tp_places():
    me = lax.axis_index("tp")
    pair, core = me // 2, me % 2
    partner = 2 * pair + (1 - core)
    cross = 2 * (1 - pair) + core
    far = 2 * (1 - pair) + (1 - core)
    return me, partner, cross, far


def aligned(start, size):
    return pl.ds(pl.multiple_of(start, size), size)


def project_kernel(count, chunk, x_ref, gain_ref, *refs):
    weights, outs = refs[:count], refs[count : 2 * count]
    wbuf, xg, nb, wsem, csend, crecv, psend, precv, fsend, frecv = refs[2 * count :]
    steps = x_ref.shape[0] // chunk
    width = x_ref.shape[1]
    peers = xg.shape[0]
    me, partner, cross, far = tp_places()
    for j in range(count):
        pltpu.make_async_copy(weights[j], wbuf.at[j], wsem.at[j]).start()
    barrier = pltpu.get_barrier_semaphore()
    for other in (partner, cross):
        pl.semaphore_signal(barrier, inc=1, device_id={"tp": other}, device_id_type=MESH)
    pl.semaphore_wait(barrier, 2)

    def hop(step, src, slot, to, send, recv):
        rows = aligned(step * chunk, chunk)
        return pltpu.make_async_remote_copy(
            src_ref=src.at[rows],
            dst_ref=xg.at[slot, rows],
            send_sem=send.at[step],
            recv_sem=recv.at[step],
            device_id={"tp": to},
            device_id_type=MESH,
        )

    for step in range(steps):
        hop(step, x_ref, me, cross, csend, crecv).start()
    for step in range(steps):
        hop(step, x_ref, me, partner, psend, precv).start()
    xg[me] = x_ref[...]

    @pl.loop(0, steps + 1)
    def _(step):
        @pl.when(step < steps)
        def _():
            hop(step, x_ref, cross, cross, csend, crecv).wait_recv()
            hop(step, xg.at[cross], cross, partner, fsend, frecv).start()

        @pl.when(step > 0)
        def _():
            now = step - 1
            hop(now, x_ref, partner, partner, psend, precv).wait_recv()
            hop(now, x_ref, far, partner, fsend, frecv).wait_recv()
            rows = aligned(now * chunk, chunk)
            total = jnp.zeros((chunk, 1), F32)
            for s in range(peers):
                piece = xg[s, rows].astype(F32)
                total = total + jnp.sum(piece * piece, axis=-1, keepdims=True)
            scale = lax.rsqrt(total / (peers * width) + EPS)
            for s in range(peers):
                cols = slice(s * width, (s + 1) * width)
                gain = gain_ref[:, cols].astype(F32)
                nb[:, cols] = (xg[s, rows].astype(F32) * scale * gain).astype(BF16)
            for j in range(count):

                @pl.when(now == 0)
                def _():
                    pltpu.make_async_copy(weights[j], wbuf.at[j], wsem.at[j]).wait()

                outs[j][rows, :] = jnp.dot(
                    nb[...], wbuf[j], preferred_element_type=F32
                ).astype(BF16)

    for step in range(steps):
        hop(step, x_ref, me, cross, csend, crecv).wait_send()
        hop(step, x_ref, me, partner, psend, precv).wait_send()
        hop(step, xg.at[cross], cross, partner, fsend, frecv).wait_send()


def project(peers, layer_input, gain, weights):
    tokens, width = layer_input.shape
    count, cols = len(weights), weights[0].shape[1]
    chunk = 256 if tokens % 256 == 0 else BLK
    steps = tokens // chunk
    vmem = pl.BlockSpec(memory_space=pltpu.VMEM)
    dma = pltpu.SemaphoreType.DMA((steps,))
    return pl.pallas_call(
        functools.partial(project_kernel, count, chunk),
        out_shape=[jax.ShapeDtypeStruct((tokens, cols), BF16)] * count,
        in_specs=[vmem, vmem] + [pl.BlockSpec(memory_space=pl.ANY)] * count,
        out_specs=[vmem] * count,
        scratch_shapes=[
            pltpu.VMEM((count,) + weights[0].shape, BF16),
            pltpu.VMEM((peers, tokens, width), BF16),
            pltpu.VMEM((chunk, peers * width), BF16),
            pltpu.SemaphoreType.DMA((count,)),
        ]
        + [dma] * 6,
        compiler_params=pltpu.CompilerParams(collective_id=0, has_side_effects=True),
        name="project",
    )(layer_input, gain, *weights)


def finish_kernel(
    heads,
    part_ref,
    shift_ref,
    pack_ref,
    start_ref,
    gate_ref,
    post_ref,
    pre_ref,
    conv_ref,
    taps_ref,
    hgain_ref,
    wr_ref,
    wc_ref,
    ogain_ref,
    out_ref,
    land,
    ent,
    back,
    halo,
    mix,
    conv,
    acc,
    pbuf,
    prcv,
    cbuf,
    crcv,
    land_state,
    s1,
    r1,
    s2,
    r2,
    hs,
    hr,
    ps,
    pr,
    cs,
    cr,
):
    tokens, width = part_ref.shape
    sp = lax.axis_size("sp")
    quarter = tokens // lax.axis_size("tp")
    half = quarter // 2
    me, partner, cross, far = tp_places()
    seq = lax.axis_index("sp")
    barrier = pltpu.get_barrier_semaphore()
    for other in (partner, cross):
        pl.semaphore_signal(barrier, inc=1, device_id={"tp": other}, device_id_type=MESH)
    for off in range(1, sp):
        pl.semaphore_signal(
            barrier, inc=1, device_id={"sp": (seq + off) % sp}, device_id_type=MESH
        )
    pl.semaphore_wait(barrier, 2 + sp - 1)

    def give(src, dst, send, recv, to):
        return pltpu.make_async_remote_copy(
            src_ref=src,
            dst_ref=dst,
            send_sem=send,
            recv_sem=recv,
            device_id=to,
            device_id_type=MESH,
        )

    def state_hop(src, dst, slot, to, send, recv):
        return give(src.at[to], dst.at[slot], send.at[to], recv.at[slot], {"sp": to})

    rim = halo.shape[1]

    def rim_hop(i, src):
        return give(
            src.at[pl.ds(tokens - rim, rim)], halo.at[i], hs.at[i], hr.at[i], {"sp": (seq + 1) % sp}
        )

    for off in range(1, sp):
        state_hop(pack_ref, land, seq, (seq + off) % sp, s1, r1).start()
    rim_hop(0, pre_ref).start()
    rim_hop(1, conv_ref).start()

    land[seq] = pack_ref[seq]
    pad = mix.shape[0] - tokens

    def fill(i):
        rows = aligned(i * quarter, quarter)
        mix[pl.ds(pl.multiple_of(pad + i * quarter, 8), quarter), :] = pre_ref[rows, :].astype(
            F32
        ) * conv_ref[rows, :].astype(F32)

    for i in range(tokens // quarter):
        fill(i)

    def convolve(i):
        rows = slice(i * quarter, (i + 1) * quarter)
        total = None
        for j in range(CK):
            first = pad + i * quarter + j - (CK - 1)
            term = mix[first : first + quarter, :] * taps_ref[j : j + 1, :].astype(F32)
            total = term if total is None else total + term
        conv[rows, :] = (post_ref[rows, :].astype(F32) * total).astype(BF16)

    for i in range(1, tokens // quarter):
        convolve(i)

    for off in range(1, sp):
        src = (seq + sp - off) % sp
        state_hop(pack_ref, land, src, (seq + off) % sp, s1, r1).wait_recv()
    running = [start_ref[h] for h in range(heads)]
    for i in range(sp):
        decays = land[i, heads]
        for h in range(heads):
            ent[i, h] = running[h]
            running[h] = decays[:, h : h + 1] * running[h] + land[i, h]
    back[seq] = ent[seq]
    for off in range(1, sp):
        state_hop(ent, back, seq, (seq + off) % sp, s2, r2).start()

    rim_hop(0, pre_ref).wait_recv()
    rim_hop(1, conv_ref).wait_recv()
    last = halo[0].astype(F32) * halo[1].astype(F32)
    mix[pad - 8 : pad, :] = jnp.where(seq > 0, last[rim - 8 :, :], 0.0)
    convolve(0)

    @pl.loop(0, tokens // quarter)
    def _(i):
        rows = aligned(i * quarter, quarter)
        acc[rows, :] = jnp.dot(conv[rows, :], wc_ref[...], preferred_element_type=F32)

    for off in range(1, sp):
        src = (seq + sp - off) % sp
        state_hop(ent, back, src, (seq + off) % sp, s2, r2).wait_recv()
    for h in range(heads):
        carried = jnp.concatenate([back[i, h] for i in range(sp)], axis=0).astype(BF16)
        land_state[h] = carried

    def mixed(which, s):
        rows = aligned(which * quarter + s * half, half)
        gated = []
        for h in range(heads):
            ch = slice(h * DV, (h + 1) * DV)
            recur = part_ref[rows, ch] + jnp.dot(
                shift_ref[rows, ch], land_state[h], preferred_element_type=F32
            )
            gate = gate_ref[rows, ch].astype(F32)
            gated.append(
                (
                    recur * rms_scale(recur) * hgain_ref[...].astype(F32) * (gate * jax.nn.sigmoid(gate))
                ).astype(BF16)
            )
        rec = jnp.concatenate(gated, axis=1)
        return acc[rows, :] + jnp.dot(rec, wr_ref[...], preferred_element_type=F32)

    def put(which, s):
        rows = aligned(which * quarter + s * half, half)
        acc[rows, :] = mixed(which, s)

    def partner_hop(i):
        return give(pbuf.at[i], prcv.at[i], ps.at[i], pr.at[i], {"tp": partner})

    def cross_hop(i):
        return give(cbuf.at[i], crcv.at[i], cs.at[i], cr.at[i], {"tp": cross})

    def share(which, s, slot):
        pbuf[slot] = mixed(which, s).astype(BF16)
        partner_hop(slot).start()

    def forward(s):
        rows = aligned(cross * quarter + s * half, half)
        partner_hop(s).wait_recv()
        cbuf[s] = (acc[rows, :] + prcv[s].astype(F32)).astype(BF16)
        cross_hop(s).start()

    share(far, 0, 0)
    put(cross, 0)
    share(far, 1, 1)
    forward(0)
    put(cross, 1)
    forward(1)
    share(partner, 0, 2)
    share(partner, 1, 3)
    put(me, 0)
    put(me, 1)
    for s in range(2):
        partner_hop(2 + s).wait_recv()
        cross_hop(s).wait_recv()
        rows = aligned(me * quarter + s * half, half)
        total = acc[rows, :] + prcv[2 + s].astype(F32) + crcv[s].astype(F32)
        out_ref[s * half : (s + 1) * half, :] = (
            total * rms_scale(total) * ogain_ref[...].astype(F32)
        ).astype(BF16)

    for off in range(1, sp):
        to = (seq + off) % sp
        state_hop(pack_ref, land, seq, to, s1, r1).wait_send()
        state_hop(ent, back, seq, to, s2, r2).wait_send()
    rim_hop(0, pre_ref).wait_send()
    rim_hop(1, conv_ref).wait_send()
    for i in range(4):
        partner_hop(i).wait_send()
    for i in range(2):
        cross_hop(i).wait_send()


def finish(sp, tp, part, shift, pack, start, gate, post, pre, convval, taps, hgain, wr, wc, ogain):
    tokens, width = part.shape
    heads = width // DV
    quarter, wide = tokens // tp, wr.shape[1]
    half = quarter // 2
    vmem = pl.BlockSpec(memory_space=pltpu.VMEM)
    pieces = (sp, heads, DK // sp, DV)
    dma = pltpu.SemaphoreType.DMA
    return pl.pallas_call(
        functools.partial(finish_kernel, heads),
        out_shape=jax.ShapeDtypeStruct((quarter, wide), BF16),
        in_specs=[vmem] * 13,
        out_specs=vmem,
        scratch_shapes=[
            pltpu.VMEM(pack.shape, F32),
            pltpu.VMEM(pieces, F32),
            pltpu.VMEM(pieces, F32),
            pltpu.VMEM((2, 16, width), BF16),
            pltpu.VMEM((tokens + 8, width), F32),
            pltpu.VMEM((tokens, width), BF16),
            pltpu.VMEM((tokens, wide), F32),
            pltpu.VMEM((4, half, wide), BF16),
            pltpu.VMEM((4, half, wide), BF16),
            pltpu.VMEM((2, half, wide), BF16),
            pltpu.VMEM((2, half, wide), BF16),
            pltpu.VMEM((heads, DK, DV), BF16),
        ]
        + [dma((sp,))] * 4
        + [dma((2,))] * 2
        + [dma((4,))] * 2
        + [dma((2,))] * 2,
        compiler_params=pltpu.CompilerParams(collective_id=1, has_side_effects=True),
        name="finish",
    )(part, shift, pack, start, gate, post, pre, convval, taps, hgain, wr, wc, ogain)


def shards(
    layer_input,
    input_norm_gain,
    query_weight,
    forget_weight,
    value_matrix,
    output_gate_weight,
    after_gate_weight,
    before_gate_weight,
    convolution_input_weight,
    forget_minimum,
    surge_log_decay,
    convolution_kernel,
    head_norm_gain,
    starting_state,
    recurrence_output_weight,
    convolution_output_weight,
    output_norm_gain,
):
    sp, tp = lax.axis_size("sp"), lax.axis_size("tp")
    weight_list = (
        query_weight,
        forget_weight,
        value_matrix,
        output_gate_weight,
        after_gate_weight,
        before_gate_weight,
        convolution_input_weight,
    )
    query_raw, forget_raw, value_raw, outgate_raw, postgate_raw, pregate_raw, convval_raw = project(
        tp, layer_input, input_norm_gain[None, :], weight_list
    )
    partial_output, shifted_query, state_pieces = local_pass(
        sp, query_raw, forget_raw, value_raw, surge_log_decay, forget_minimum[None, :]
    )
    return finish(
        sp,
        tp,
        partial_output,
        shifted_query,
        state_pieces,
        starting_state,
        outgate_raw,
        postgate_raw,
        pregate_raw,
        convval_raw,
        convolution_kernel,
        head_norm_gain[None, :],
        recurrence_output_weight,
        convolution_output_weight,
        output_norm_gain[None, :],
    )


def solution(mesh):
    return jax.shard_map(
        shards,
        mesh=mesh,
        in_specs=(
            P("sp", "tp"),
            P(),
            P(None, "tp"),
            P(None, "tp"),
            P(None, "tp"),
            P(None, "tp"),
            P(None, "tp"),
            P(None, "tp"),
            P(None, "tp"),
            P("tp"),
            P("sp", "tp"),
            P(None, "tp"),
            P(),
            P("tp", "sp", None),
            P("tp", None),
            P("tp", None),
            P(),
        ),
        out_specs=P(("sp", "tp"), None),
        check_vma=False,
    )
```

time: 186 us -> 95.9 us (0.52)
  Pallas kernels: 9.96 us -> 91.6 us
  waiting for transfers between devices: 75.8 us -> 0 us
  matrix products: 43.8 us -> 0 us
  starting transfers between devices: 16.4 us -> 0 us
  between operations: 13.5 us -> 0.04 us
  other arithmetic: 13.2 us -> 0 us
  local copies, waits for them, and re-layouts: 12.4 us -> 3.99 us
    pallas_call x0 -> x2, Pallas kernels: none -> 81.5 us  [the longest x1 45.8 us: finish(): pl.pallas_call(functools.partial(finish_kernel, heads), out_shape=jax.Sha...]
    dot_general x8 -> x0, matrix products: 43.8 us -> none  [the longest x5 20.9 us: shards(): jnp.dot(normed, weight, preferred_element_type=jnp.float32)]
    reduce_scatter x1 -> x0, waiting for transfers between devices: 36.4 us -> none  [shards(): lax.psum_scatter((jnp.dot(rec_out, recurrence_output_weight, preferred_el...]
    all_gather x1 -> x0, waiting for transfers between devices: 30.8 us -> none  [shards(): collected_rows = lax.all_gather(layer_input, 'tp', axis=1, tiled=True)]
    all_to_all x3 -> x0, starting transfers between devices: 12.3 us -> none  [the longest x1 5.52 us: shards(): lax.all_to_all(local_total[None, :, :, None], 'sp', split_axis=2, concat_...]
    all_to_all x3 -> x0, waiting for transfers between devices: 7.86 us -> none  [the longest x1 5.03 us: shards(): lax.all_to_all(local_total[None, :, :, None], 'sp', split_axis=2, concat_...]
    reshape x2 -> x0, local copies, waits for them, and re-layouts: 6.09 us -> none  [the longest x1 3.08 us: shards(): partial_output.reshape(tokens_dev, heads_local, DV)]
    reduce_sum x2 -> x0, other arithmetic: 4.09 us -> none  [rms_scale(): jnp.mean(value_rows * value_rows, axis=-1, keepdims=True) + EPS]
  transfers between devices with their start and end apart: 6 -> 0, of which waited for: 4 -> 0; matrix products, arithmetic and copies ran while one was open for 19% -> 0% of each run, Pallas kernels for 0% -> 0%
where the time goes in v2:
time: 95.9 us; the launch traced here: 95.6 us
  Pallas kernels  91.6 us (96%)
  local copies, waits for them, and re-layouts  3.99 us (4%)
    pallas_call x1, Pallas kernels, finish(): pl.pallas_call(functools.partial(finish_kernel, heads), out_shape=jax.Sha...  45.8 us
    pallas_call x1, Pallas kernels, project(): pl.pallas_call(functools.partial(project_kernel, count, chunk), out_shape...  35.8 us
    pallas_call x1, Pallas kernels, local_pass(): pl.pallas_call(functools.partial(local_kernel, heads), grid=(tokens // ro...  10 us
    unnamed x3, local copies, waits for them, and re-layouts  2.1 us

profile of v2, /device:TPU:0, one launch (start us, length us, event | category | flops | bytes accessed | tf_op | source)
XLA Modules:
  0.0 95.6 jit_solution(7117009957982537997)
XLA Ops:
  0.0 1.3 %broadcast_in_dim.12.gain_ref = bf16[1,2048]{1,0:T(2,128)(2,1)} reshape(bf16[2048]{0:T(1024)(128)(2,1)} %param.18) | data formatting | bytes 8192 | tf_op jit(solution)/shard_map/broadcast_in_dim | solution.py:497
  1.3 35.8 %project.1 = (bf16[768,512]{1,0:T(8,128)(2,1)}, bf16[768,512]{1,0:T(8,128)(2,1)}, bf16[768,512]{1,0:T(8,128)(2,1)}, bf16[768,512]{1,0:T(8,128)(2,1)}, bf16[768,5...) custom-call(bf16[768,512]{1,0:T(8,128)(2,1)} %x_ref.1, ...), custom_call_target="tpu_custom_call" | custom-call | tf_op jit(solution)/shard_map/project/pallas_call | solution.py:212
  37.1 0.0 copy-start
  37.1 10.0 %local_pass.1 = (f32[768,512]{1,0:T(8,128)}, bf16[768,512]{1,0:T(8,128)(2,1)}, f32[8,5,16,128]{3,2,1,0:T(8,128)}) custom-call(bf16[768,512]{1,0:T(8,128)(2,1)} %get-tuple-element.15.q_ref, bf16[768,512]{1,0:T(8,128)(2,1)} %get-tuple-element.16.f_ref, bf16[768,512]{1,0:T(8,128)(2,1)} %get-tuple-element.17.v_ref, f32[768,512]{1,0:T(8,128)} %surge_ref.1, ...), custom_call_target="tpu_custom_call" | custom-call | flops 393216000 | bytes 6291456 | tf_op jit(solution)/shard_map/local_pass/pallas_call | solution.py:101
  47.1 0.0 copy-done
  47.2 0.6 broadcast_in_dim.15.ogain_ref
  47.8 45.8 %finish.1 = bf16[192,2048]{1,0:T(8,128)(2,1)} custom-call(f32[768,512]{1,0:T(8,128)} %get-tuple-element.18.part_ref, bf16[768,512]{1,0:T(8,128)(2,1)} %get-tuple-element.19.shift_ref, f32[8,5,16,128]{3,2,1,0:T(8,128)} %get-tuple-element.20.pack_ref, f32[4,16,128]{2,1,0:T(8,128)} %start_ref.1, bf16[768,512]{1,0:T(8,128)(2,1)} %get-tuple-element.21.gate_ref, ...), custom_call_target="tpu_custom_call" | custom-call | tf_op jit(solution)/shard_map/finish/pallas_call | solution.py:439
  93.5 2.1 %copy.19 = bf16[192,2048]{1,0:T(8,128)(2,1)} copy(bf16[192,2048]{1,0:T(8,128)(2,1)} %finish.1) | data formatting | bytes 1572864
Async XLA Ops:
  37.1 10.1 %copy-start = (bf16[2048]{0:T(1024)(128)(2,1)S(1)}, bf16[2048]{0:T(1024)(128)(2,1)}, u32[]{:S(2)}) copy-start(bf16[2048]{0:T(1024)(128)(2,1)} %param.33) | copy-start | bytes 12292

commit v3 on v2

--- a/solution.py
+++ b/solution.py
@@ -11,7 +11,7 @@
 DV = 128
 CK = 3
 BLK = 64
-ROWS = 128
+ROWS = 256
 
 
 EPS = 1e-06
@@ -33,7 +33,7 @@
 
 
 def local_kernel(
-    heads, q_ref, f_ref, v_ref, surge_ref, fmin_ref, part_ref, shift_ref, pack_ref, st, run
+    heads, q_ref, f_ref, v_ref, surge_ref, fmin_ref, part_ref, shift_ref, pack_ref, decay_ref, st, run
 ):
     step = pl.program_id(0)
 
@@ -45,13 +45,19 @@
     row = lax.broadcasted_iota(jnp.int32, (BLK, BLK), 0)
     col = lax.broadcasted_iota(jnp.int32, (BLK, BLK), 1)
     causal = col <= row
-    middle = (causal.astype(F32) - (col < BLK // 2).astype(F32))
+    middle = (causal.astype(F32) - (col < BLK // 2).astype(F32)).astype(BF16)
+    middle = jnp.concatenate([middle] * 3, axis=1)
     for b in range(q_ref.shape[0] // BLK):
         rows = slice(b * BLK, (b + 1) * BLK)
         forget = f_ref[rows, :].astype(F32)
         keys = (1.0 - fmin_ref[...]) * jax.nn.sigmoid(-forget)
         logs = jnp.log1p(-keys) + surge_ref[rows, :]
-        rel = jnp.dot(middle, logs, precision=lax.Precision.HIGHEST, preferred_element_type=F32)
+        high = logs.astype(BF16)
+        rest = logs - high.astype(F32)
+        next_term = rest.astype(BF16)
+        low = (rest - next_term.astype(F32)).astype(BF16)
+        terms = jnp.concatenate([high, next_term, low], axis=0)
+        rel = jnp.dot(middle, terms, preferred_element_type=F32)
         mid = logs[0:1, :] - rel[0:1, :]
         tail = rel[BLK - 1 : BLK, :]
         raw = q_ref[rows, :].astype(F32)
@@ -87,9 +93,9 @@
             state = st[h].T
             decays = jnp.where(lane == h, jnp.broadcast_to(whole[:, ch], (DV, DK)).T, decays)
             for p in range(peers):
-                pack_ref[p, h] = state[p * piece : (p + 1) * piece]
+                pack_ref[p, h] = state[p * piece : (p + 1) * piece].astype(BF16)
         for p in range(peers):
-            pack_ref[p, heads] = decays[p * piece : (p + 1) * piece]
+            decay_ref[p] = decays[p * piece : (p + 1) * piece]
 
 
 def local_pass(peers, query_raw, forget_raw, value_raw, surge, fmin):
@@ -105,12 +111,14 @@
         out_specs=[
             tile,
             tile,
-            pl.BlockSpec((peers, heads + 1, DK // peers, DV), lambda i: (0, 0, 0, 0)),
+            pl.BlockSpec((peers, heads, DK // peers, DV), lambda i: (0, 0, 0, 0)),
+            pl.BlockSpec((peers, DK // peers, DV), lambda i: (0, 0, 0)),
         ],
         out_shape=[
             jax.ShapeDtypeStruct((tokens, width), F32),
             jax.ShapeDtypeStruct((tokens, width), BF16),
-            jax.ShapeDtypeStruct((peers, heads + 1, DK // peers, DV), F32),
+            jax.ShapeDtypeStruct((peers, heads, DK // peers, DV), BF16),
+            jax.ShapeDtypeStruct((peers, DK // peers, DV), F32),
         ],
         scratch_shapes=[pltpu.VMEM((heads, DV, DK), F32), pltpu.VMEM((1, width), F32)],
         cost_estimate=pl.CostEstimate(
@@ -231,6 +239,7 @@
     part_ref,
     shift_ref,
     pack_ref,
+    decay_ref,
     start_ref,
     gate_ref,
     post_ref,
@@ -243,6 +252,7 @@
     ogain_ref,
     out_ref,
     land,
+    land_decay,
     ent,
     back,
     halo,
@@ -256,6 +266,8 @@
     land_state,
     s1,
     r1,
+    sd,
+    rd,
     s2,
     r2,
     hs,
@@ -301,11 +313,13 @@
         )
 
     for off in range(1, sp):
+        state_hop(decay_ref, land_decay, seq, (seq + off) % sp, sd, rd).start()
         state_hop(pack_ref, land, seq, (seq + off) % sp, s1, r1).start()
     rim_hop(0, pre_ref).start()
     rim_hop(1, conv_ref).start()
 
     land[seq] = pack_ref[seq]
+    land_decay[seq] = decay_ref[seq]
     pad = mix.shape[0] - tokens
 
     def fill(i):
@@ -331,13 +345,14 @@
 
     for off in range(1, sp):
         src = (seq + sp - off) % sp
+        state_hop(decay_ref, land_decay, src, (seq + off) % sp, sd, rd).wait_recv()
         state_hop(pack_ref, land, src, (seq + off) % sp, s1, r1).wait_recv()
     running = [start_ref[h] for h in range(heads)]
     for i in range(sp):
-        decays = land[i, heads]
+        decays = land_decay[i]
         for h in range(heads):
-            ent[i, h] = running[h]
-            running[h] = decays[:, h : h + 1] * running[h] + land[i, h]
+            ent[i, h] = running[h].astype(BF16)
+            running[h] = decays[:, h : h + 1] * running[h] + land[i, h].astype(F32)
     back[seq] = ent[seq]
     for off in range(1, sp):
         state_hop(ent, back, seq, (seq + off) % sp, s2, r2).start()
@@ -357,7 +372,7 @@
         src = (seq + sp - off) % sp
         state_hop(ent, back, src, (seq + off) % sp, s2, r2).wait_recv()
     for h in range(heads):
-        carried = jnp.concatenate([back[i, h] for i in range(sp)], axis=0).astype(BF16)
+        carried = jnp.concatenate([back[i, h].astype(F32) for i in range(sp)], axis=0).astype(BF16)
         land_state[h] = carried
 
     def mixed(which, s):
@@ -418,6 +433,7 @@
 
     for off in range(1, sp):
         to = (seq + off) % sp
+        state_hop(decay_ref, land_decay, seq, to, sd, rd).wait_send()
         state_hop(pack_ref, land, seq, to, s1, r1).wait_send()
         state_hop(ent, back, seq, to, s2, r2).wait_send()
     rim_hop(0, pre_ref).wait_send()
@@ -428,7 +444,7 @@
         cross_hop(i).wait_send()
 
 
-def finish(sp, tp, part, shift, pack, start, gate, post, pre, convval, taps, hgain, wr, wc, ogain):
+def finish(sp, tp, part, shift, pack, decay, start, gate, post, pre, convval, taps, hgain, wr, wc, ogain):
     tokens, width = part.shape
     heads = width // DV
     quarter, wide = tokens // tp, wr.shape[1]
@@ -439,12 +455,13 @@
     return pl.pallas_call(
         functools.partial(finish_kernel, heads),
         out_shape=jax.ShapeDtypeStruct((quarter, wide), BF16),
-        in_specs=[vmem] * 13,
+        in_specs=[vmem] * 14,
         out_specs=vmem,
         scratch_shapes=[
-            pltpu.VMEM(pack.shape, F32),
-            pltpu.VMEM(pieces, F32),
-            pltpu.VMEM(pieces, F32),
+            pltpu.VMEM(pieces, BF16),
+            pltpu.VMEM(decay.shape, F32),
+            pltpu.VMEM(pieces, BF16),
+            pltpu.VMEM(pieces, BF16),
             pltpu.VMEM((2, 16, width), BF16),
             pltpu.VMEM((tokens + 8, width), F32),
             pltpu.VMEM((tokens, width), BF16),
@@ -455,13 +472,13 @@
             pltpu.VMEM((2, half, wide), BF16),
             pltpu.VMEM((heads, DK, DV), BF16),
         ]
-        + [dma((sp,))] * 4
+        + [dma((sp,))] * 6
         + [dma((2,))] * 2
         + [dma((4,))] * 2
         + [dma((2,))] * 2,
         compiler_params=pltpu.CompilerParams(collective_id=1, has_side_effects=True),
         name="finish",
-    )(part, shift, pack, start, gate, post, pre, convval, taps, hgain, wr, wc, ogain)
+    )(part, shift, pack, decay, start, gate, post, pre, convval, taps, hgain, wr, wc, ogain)
 
 
 def shards(
@@ -496,7 +513,7 @@
     query_raw, forget_raw, value_raw, outgate_raw, postgate_raw, pregate_raw, convval_raw = project(
         tp, layer_input, input_norm_gain[None, :], weight_list
     )
-    partial_output, shifted_query, state_pieces = local_pass(
+    partial_output, shifted_query, state_pieces, state_decays = local_pass(
         sp, query_raw, forget_raw, value_raw, surge_log_decay, forget_minimum[None, :]
     )
     return finish(
@@ -505,6 +522,7 @@
         partial_output,
         shifted_query,
         state_pieces,
+        state_decays,
         starting_state,
         outgate_raw,
         postgate_raw,

time: 95.9 us -> 91.6 us (0.955)
  Pallas kernels: 91.6 us -> 87.3 us
    pallas_call x1, Pallas kernels: 45.8 us -> 42.9 us  [finish(): pl.pallas_call(functools.partial(finish_kernel, heads), out_shape=jax.Sha...]
    pallas_call x1, Pallas kernels: 10 us -> 8.64 us  [local_pass(): pl.pallas_call(functools.partial(local_kernel, heads), grid=(tokens // ro...]
where the time goes in v3:
time: 91.6 us; the launch traced here: 91.4 us
  Pallas kernels  87.3 us (95%)
  local copies, waits for them, and re-layouts  3.99 us (4%)
    pallas_call x1, Pallas kernels, finish(): pl.pallas_call(functools.partial(finish_kernel, heads), out_shape=jax.Sha...  42.9 us
    pallas_call x1, Pallas kernels, project(): pl.pallas_call(functools.partial(project_kernel, count, chunk), out_shape...  35.8 us
    pallas_call x1, Pallas kernels, local_pass(): pl.pallas_call(functools.partial(local_kernel, heads), grid=(tokens // ro...  8.64 us
    unnamed x3, local copies, waits for them, and re-layouts  2.1 us

profile of v3, /device:TPU:0, one launch (start us, length us, event | category | flops | bytes accessed | tf_op | source)
XLA Modules:
  0.0 91.4 jit_solution(165502501147594104)
XLA Ops:
  0.0 1.3 %broadcast_in_dim.12.gain_ref = bf16[1,2048]{1,0:T(2,128)(2,1)} reshape(bf16[2048]{0:T(1024)(128)(2,1)} %param.18) | data formatting | bytes 8192 | tf_op jit(solution)/shard_map/broadcast_in_dim | solution.py:514
  1.3 35.8 %project.1 = (bf16[768,512]{1,0:T(8,128)(2,1)}, bf16[768,512]{1,0:T(8,128)(2,1)}, bf16[768,512]{1,0:T(8,128)(2,1)}, bf16[768,512]{1,0:T(8,128)(2,1)}, bf16[768,5...) custom-call(bf16[768,512]{1,0:T(8,128)(2,1)} %x_ref.1, ...), custom_call_target="tpu_custom_call" | custom-call | tf_op jit(solution)/shard_map/project/pallas_call | solution.py:220
  37.1 0.0 copy-start
  37.1 8.6 %local_pass.1 = (f32[768,512]{1,0:T(8,128)}, bf16[768,512]{1,0:T(8,128)(2,1)}, bf16[8,4,16,128]{3,2,1,0:T(8,128)(2,1)}, f32[8,16,128]{2,1,0:T(8,128)}) custom-call(bf16[768,512]{1,0:T(8,128)(2,1)} %get-tuple-element.16.q_ref, bf16[768,512]{1,0:T(8,128)(2,1)} %get-tuple-element.17.f_ref, bf16[768,512]{1,0:T(8,128)(2,1)} %get-tuple-element.18.v_ref, ...), custom_call_target="tpu_custom_call" | custom-call | flops 393216000 | bytes 6291456 | tf_op jit(solution)/shard_map/local_pass/pallas_call | solution.py:107
  45.7 0.0 copy-done
  45.8 0.6 broadcast_in_dim.15.ogain_ref
  46.4 42.9 %finish.1 = bf16[192,2048]{1,0:T(8,128)(2,1)} custom-call(f32[768,512]{1,0:T(8,128)} %get-tuple-element.19.part_ref, bf16[768,512]{1,0:T(8,128)(2,1)} %get-tuple-element.20.shift_ref, bf16[8,4,16,128]{3,2,1,0:T(8,128)(2,1)} %get-tuple-element.21.pack_ref, f32[8,16,128]{2,1,0:T(8,128)} %get-tuple-element.22.decay_ref, f32[4,16,128]{2,1,0:T(8,128)} %start_ref.1, ...), custom_call_target="tpu_custom_call" | custom-call | tf_op jit(solution)/shard_map/finish/pallas_call | solution.py:455
  89.3 2.1 %copy.19 = bf16[192,2048]{1,0:T(8,128)(2,1)} copy(bf16[192,2048]{1,0:T(8,128)(2,1)} %finish.1) | data formatting | bytes 1572864
Async XLA Ops:
  37.1 8.7 %copy-start = (bf16[2048]{0:T(1024)(128)(2,1)S(1)}, bf16[2048]{0:T(1024)(128)(2,1)}, u32[]{:S(2)}) copy-start(bf16[2048]{0:T(1024)(128)(2,1)} %param.33) | copy-start | bytes 12292
